TPU v7x, 32 devices: a whole 2x2x4 slice. The times are simulated.
32 devices in a mesh: ep: 8 (over z, x), tp: 4 (over y, core).
Axes of the slice: x: 2, y: 2, z: 4, core: 2. Of those that a mesh axis runs over, the one named last changes fastest.
Arguments:
- tokens_first: bfloat16 [4096, 2048], P('ep'), may hold values from -6 to 6
- attn_gain: float32 [2048], replicated, may hold values from 0.1 to 1.9
- w_query: bfloat16 [2048, 1024], P(None, 'tp'), may hold values from -6 to 6
- key_matrix: bfloat16 [2048, 512], P(None, 'tp'), may hold values from -6 to 6
- value_matrix: bfloat16 [2048, 512], P(None, 'tp'), may hold values from -0.125 to 0.125
- head_sink_logit: float32 [16], P('tp'), may hold values from 1 to 5
- w_output: bfloat16 [1024, 2048], P('tp'), may hold values from -0.75 to 0.75
- tokens_second: bfloat16 [1024, 2048], P('ep'), may hold values from -6 to 6
- ffn_gain: float32 [2048], replicated, may hold values from 0.1 to 1.9
- routes: int32 [1024, 4], P('ep'), may hold values from 0 to 15, all different within a row; in each aligned block of 128 rows (0 to 127, 128 to 255, ...) at most 64 rows name the same one
- route_weight: float32 [1024, 4], P('ep'), may hold values from 0.2 to 1.5
- w_gate_exp: bfloat16 [16, 2048, 2048], P('ep', None, 'tp'), may hold values from -0.125 to 0.125
- w_up_exp: bfloat16 [16, 2048, 2048], P('ep', None, 'tp'), may hold values from -0.125 to 0.125
- w_down_exp: bfloat16 [16, 2048, 2048], P('ep', 'tp'), may hold values from -0.125 to 0.125
- w_gate_shared: bfloat16 [2048, 1024], P(None, 'tp'), may hold values from -0.125 to 0.125
- w_up_shared: bfloat16 [2048, 1024], P(None, 'tp'), may hold values from -0.125 to 0.125
- w_down_shared: bfloat16 [1024, 2048], P('tp'), may hold values from -0.1875 to 0.1875
Outputs:
- mixer_out: bfloat16 [4096, 2048], P(('ep', 'tp'))
- moe_out: bfloat16 [1024, 2048], P('ep', 'tp')
Inputs may be any that keep to these rules, and one draw needn't show every extreme that they name: `routes`: each row names 4 different experts; among the rows of one index of ep no expert is named more than 64 times, a bound that some block reaches.
All inputs are finite; a program needn't handle non-finite values.
Results may differ from a plain program's by a relative error of at most 0.017.
Values may be sent and summed in bfloat16 or wider, within the bound.
No kernel may reach another device: no remote copies, remote signals or barrier semaphores. Data moves between devices by JAX's collectives and lax.ppermute only.
A program may use at most 64 MiB of HBM per device.

v0:
```python
import jax
import jax.numpy as jnp
from jax import lax
from jax.sharding import PartitionSpec as P

MODEL_WIDTH = 2048
HEAD_SIZE = 64
BAND_LENGTH = 128
rope_base = 10000.0
norm_eps = 1e-06


def from_behind(value, axis, by):
    devices = lax.axis_size(axis)
    pairs = [(i, i + by) for i in range(devices) if 0 <= i + by < devices]
    return lax.ppermute(value, axis, pairs)


def rms_scale(inputs, gain):
    wide = inputs.astype(jnp.float32)
    scaled = wide * lax.rsqrt(jnp.mean(wide * wide, axis=-1, keepdims=True) + norm_eps)
    return (scaled * gain).astype(jnp.bfloat16)


def apply_rotary(heads, token_positions):
    freqs = rope_base ** (-jnp.arange(0, HEAD_SIZE, 2, dtype=jnp.float32) / HEAD_SIZE)
    angles = token_positions[:, None] * freqs[None, :]
    cosine = jnp.cos(angles)[:, None, :]
    sine = jnp.sin(angles)[:, None, :]
    first_half, second_half = jnp.split(heads, 2, axis=-1)
    return jnp.concatenate(
        [first_half * cosine - second_half * sine, second_half * cosine + first_half * sine],
        axis=-1,
    )


def local(
    tokens_first,
    attn_gain,
    w_query,
    key_matrix,
    value_matrix,
    head_sink_logit,
    w_output,
    tokens_second,
    ffn_gain,
    routes,
    route_weight,
    w_gate_exp,
    w_up_exp,
    w_down_exp,
    w_gate_shared,
    w_up_shared,
    w_down_shared,
):
    rows_first = tokens_first.shape[0]
    norm_input = rms_scale(tokens_first, attn_gain)
    offset = lax.axis_index("ep") * rows_first
    token_positions = (offset + jnp.arange(rows_first, dtype=jnp.int32)).astype(jnp.float32)
    head_count = w_query.shape[1] // HEAD_SIZE
    key_heads = key_matrix.shape[1] // HEAD_SIZE
    head_group = head_count // key_heads
    query_rows = apply_rotary(
        jnp.dot(norm_input, w_query, preferred_element_type=jnp.float32).reshape(
            rows_first, head_count, HEAD_SIZE
        ),
        token_positions,
    ).astype(jnp.bfloat16)
    keys_local = apply_rotary(
        jnp.dot(norm_input, key_matrix, preferred_element_type=jnp.float32).reshape(
            rows_first, key_heads, HEAD_SIZE
        ),
        token_positions,
    ).astype(jnp.bfloat16)
    values_local = (
        jnp.dot(norm_input, value_matrix, preferred_element_type=jnp.float32)
        .astype(jnp.bfloat16)
        .reshape(rows_first, key_heads, HEAD_SIZE)
    )
    keys_before, values_before = from_behind(
        (keys_local[rows_first - BAND_LENGTH :], values_local[rows_first - BAND_LENGTH :]), "ep", 1
    )
    keys_all = jnp.concatenate([keys_before, keys_local], axis=0)
    values_all = jnp.concatenate([values_before, values_local], axis=0)
    layer_block = min(512, rows_first)
    sink_scores = head_sink_logit.reshape(key_heads, head_group)[:, :, None, None]

    def attend(index):
        leading_row = index * layer_block
        block_queries = query_rows.reshape(layer_block, key_heads, head_group, HEAD_SIZE)
        scores = jnp.einsum(
            "qhgd,khd->hgqk", block_queries, keys_all, preferred_element_type=jnp.float32
        ) * HEAD_SIZE ** (-0.5)
        query_pos = offset + leading_row + jnp.arange(layer_block, dtype=jnp.int32)
        key_pos = (
            offset
            + leading_row
            - BAND_LENGTH
            + jnp.arange(layer_block + BAND_LENGTH, dtype=jnp.int32)
        )
        offsets = query_pos[:, None] - key_pos[None, :]
        visible = (offsets >= 0) & (offsets < BAND_LENGTH) & (key_pos[None, :] >= 0)
        scores = jnp.where(visible[None, None], scores, -jnp.inf)
        peak = jnp.maximum(jnp.max(scores, axis=-1, keepdims=True), sink_scores)
        expo = jnp.exp(scores - peak)
        total = jnp.sum(expo, axis=-1, keepdims=True) + jnp.exp(sink_scores - peak)
        weights = (expo / total).astype(jnp.bfloat16)
        mixed = jnp.einsum(
            "hgqk,khd->qhgd", weights, values_all, preferred_element_type=jnp.float32
        )
        return mixed.astype(jnp.bfloat16).reshape(layer_block, head_count * HEAD_SIZE)

    attended = lax.map(attend, jnp.arange(rows_first // layer_block, dtype=jnp.int32)).reshape(
        rows_first, head_count * HEAD_SIZE
    )
    mixer_out = lax.psum_scatter(
        jnp.dot(attended, w_output, preferred_element_type=jnp.float32).astype(jnp.bfloat16),
        "tp",
        scatter_dimension=0,
        tiled=True,
    )
    rows_second = tokens_second.shape[0]
    topk = routes.shape[1]
    exp_dev = w_gate_exp.shape[0]
    n_expdev = lax.axis_size("ep")
    experts = exp_dev * n_expdev
    capacity = max(2, 2 * rows_second * topk // experts)
    slot_count = experts * capacity
    normed_second = rms_scale(tokens_second, ffn_gain)
    flat = routes.reshape(-1)
    onehot = (flat[:, None] == jnp.arange(experts, dtype=jnp.int32)[None, :]).astype(jnp.int32)
    ranks = jnp.sum((jnp.cumsum(onehot, axis=0) - onehot) * onehot, axis=1)
    slots = flat * capacity + ranks
    match = (jnp.arange(slot_count, dtype=jnp.int32)[:, None] == slots[None, :]).reshape(
        slot_count, rows_second, topk
    )
    dispatch = jnp.sum(match.astype(jnp.float32), axis=2).astype(jnp.bfloat16)
    combine = jnp.sum(match.astype(jnp.float32) * route_weight[None, :, :], axis=2)
    width = normed_second.shape[1] // lax.axis_size("tp")
    feature_slice = lax.dynamic_slice_in_dim(normed_second, lax.axis_index("tp") * width, width, 1)
    outgoing = jnp.dot(dispatch, feature_slice, preferred_element_type=jnp.float32).astype(
        jnp.bfloat16
    )
    arrived = lax.all_to_all(outgoing, "ep", split_axis=0, concat_axis=0, tiled=True)
    piece = lax.all_gather(arrived, "tp", axis=1, tiled=True)
    cols = piece.shape[1]
    part = piece.reshape(n_expdev, exp_dev, capacity, cols)
    gate_pre = jnp.einsum("sjcd,jdf->sjcf", part, w_gate_exp, preferred_element_type=jnp.float32)
    up_pre = jnp.einsum("sjcd,jdf->sjcf", part, w_up_exp, preferred_element_type=jnp.float32)
    hidden = (jax.nn.silu(gate_pre) * up_pre).astype(jnp.bfloat16)
    shared_hidden = (
        jax.nn.silu(jnp.dot(normed_second, w_gate_shared, preferred_element_type=jnp.float32))
        * jnp.dot(normed_second, w_up_shared, preferred_element_type=jnp.float32)
    ).astype(jnp.bfloat16)
    routed_term = jnp.einsum(
        "sjcf,jfd->dsjc", hidden, w_down_exp, preferred_element_type=jnp.float32
    ).reshape(lax.axis_size("tp") * (MODEL_WIDTH // lax.axis_size("tp")), slot_count)
    shared_term = lax.dot_general(
        w_down_shared, shared_hidden, (((0,), (1,)), ((), ())), preferred_element_type=jnp.float32
    )
    summed = lax.psum_scatter(
        jnp.concatenate([routed_term, shared_term], axis=1).astype(jnp.bfloat16),
        "tp",
        scatter_dimension=0,
        tiled=True,
    ).astype(jnp.float32)
    routed_part = summed[:, :slot_count].astype(jnp.bfloat16)
    returned = lax.all_to_all(routed_part, "ep", split_axis=1, concat_axis=1, tiled=True)
    weighted = lax.dot_general(
        combine,
        returned.astype(jnp.float32),
        (((0,), (1,)), ((), ())),
        precision=lax.Precision.HIGHEST,
    )
    moe_out = (weighted + summed[:, slot_count:].T).astype(jnp.bfloat16)
    return (mixer_out, moe_out)


def solution(mesh):
    in_specs = (
        P("ep", None),
        P(),
        P(None, "tp"),
        P(None, "tp"),
        P(None, "tp"),
        P("tp"),
        P("tp", None),
        P("ep", None),
        P(),
        P("ep", None),
        P("ep", None),
        P("ep", None, "tp"),
        P("ep", None, "tp"),
        P("ep", "tp", None),
        P(None, "tp"),
        P(None, "tp"),
        P("tp", None),
    )
    out_specs = (P(("ep", "tp"), None), P("ep", "tp"))
    return jax.shard_map(local, mesh=mesh, in_specs=in_specs, out_specs=out_specs, check_vma=False)
```

profile of v0, /device:TPU:0, one launch (start us, length us, event | category | flops | bytes accessed | tf_op | source)
XLA Modules:
  0.0 194.5 jit_solution(10042323882435477261)
XLA Ops:
  7.2 0.0 copy-start
  7.2 0.0 all-gather.2.cloned.1.call-start
  7.2 0.9 copy.42
  8.2 0.1 eq.40
  8.3 0.1 eq.44
  8.4 1.2 reduce-window.6
  9.5 0.2 slice_reduce_fusion
  9.8 0.1 fusion.58
  9.9 0.1 reduce_sum.60
  10.0 0.1 copy.45
  10.1 0.7 multiply_add_fusion
  10.8 1.2 fusion.34
  12.0 1.2 convert_reduce_fusion
  13.2 1.2 fusion.36
  14.4 0.4 convolution_convert_fusion.2
  14.9 32.9 %all_to_all.24 = bf16[8,128,512]{2,1,0:T(8,128)(2,1)} all-to-all(bf16[8,128,512]{2,1,0:T(8,128)(2,1)S(1)} %bitcast.121), channel_id=1, replica_groups=mesh['ep'=8,'tp'=4] {'ep'}, dimensions={0} | all-to-all | bytes 2097152 | tf_op jit(solution)/shard_map/all_to_all | solution.py:144
  47.8 0.0 all-gather.2.cloned.1.call-update
  47.8 0.0 reduce-scatter.5.cloned.1.call-start
  47.9 0.3 fusion.73
  48.2 2.3 %fusion.16 = bf16[2048,128]{0,1:T(8,128)(2,1)S(1)} fusion(bf16[256,2048]{1,0:T(8,128)(2,1)} %param.33, bf16[128,2048]{1,0:T(8,128)(2,1)S(1)} %fusion.36, bf16[2048,256]{1,0:T(8,128)(2,1)} %param.32, f32[128,256]{1,0:T(8,128)S(1)} %fusion.73), kind=kOutput, calls=%fused_computation.23 | convolution fusion | flops 268894208 | bytes 3276800 | tf_op jit(solution)/shard_map/dot_general | solution.py:158
  50.5 30.9 %all-gather.2.cloned.1.call-done = bf16[1024,2048]{1,0:T(8,128)(2,1)} async-done(((bf16[1024,512]{1,0:T(8,128)(2,1)}), bf16[1024,2048]{1,0:T(8,128)(2,1)}) %all-gather.2.cloned.1.call-update) | async-done | bytes 4194320 | tf_op jit(solution)/shard_map/all_gather | solution.py:145
  81.5 7.2 %fusion.8 = f32[2,8,64,512]{3,2,1,0:T(8,128)} fusion(bf16[2,2048,512]{2,1,0:T(8,128)(2,1)} %param.28, bf16[8,2,64,2048]{3,2,1,0:T(8,128)(2,1)} %bitcast.130), kind=kOutput, calls=%fused_computation.14 | convolution fusion | flops 2147483648 | bytes 10485760 | tf_op jit(solution)/shard_map/sjcd,jdf->sjcf/dot_general | solution.py:148
  88.7 11.8 %convert_bitcast_fusion = bf16[2048,8,2,64]{0,3,1,2:T(8,128)(2,1)} fusion(bf16[2,512,2048]{2,1,0:T(8,128)(2,1)} %param.30, f32[2,8,64,512]{3,2,1,0:T(8,128)} %fusion.8, bf16[2,2048,512]{2,1,0:T(8,128)(2,1)} %param.29, bf16[8,2,64,2048]{3,2,1,0:T(8,128)(2,1)} %bitcast.131), kind=kOutput, calls=%fused_computation.16 | convolution fusion | flops 4300210176 | bytes 18874368 | tf_op jit(solution)/shard_map/sjcf,jfd->dsjc/dot_general | solution.py:155
  100.5 2.5 %copy.48 = bf16[2048,8,2,64]{0,3,2,1:T(8,128)(2,1)S(1)} copy(bf16[2048,8,2,64]{0,3,1,2:T(8,128)(2,1)} %convert_bitcast_fusion) | data formatting | bytes 8388608 | tf_op jit(solution)/shard_map/sjcf,jfd->dsjc/transpose | solution.py:155
  103.0 2.5 %pad_maximum_fusion = bf16[2048,1152]{0,1:T(8,128)(2,1)} fusion(bf16[2048,128]{0,1:T(8,128)(2,1)S(1)} %fusion.16, bf16[2048,1024]{0,1:T(8,128)(2,1)S(1)} %bitcast.118), kind=kLoop, calls=%fused_computation.5 | loop fusion | flops 9437184 | bytes 9437184 | tf_op jit(solution)/shard_map/concatenate | solution.py:162
  105.5 0.0 reduce-scatter.5.cloned.1.call-update
  105.5 0.0 reduce-scatter.3.cloned.1.call-start
  105.6 2.2 %fusion.1 = f32[512]{0:T(512)S(1)} fusion(bf16[512,2048]{1,0:T(8,128)(2,1)} %param.17), kind=kLoop, calls=%fused_computation.7 | loop fusion | flops 3145216 | bytes 2099200 | tf_op jit(solution)/shard_map/reduce_sum | solution.py:21
  107.9 0.3 multiply_cosine_fusion
  108.2 2.6 %fusion.70 = f32[512,128]{0,1:T(8,128)S(1)} fusion(bf16[2048,128]{1,0:T(8,128)(2,1)S(1)} %copy-done.4, bf16[512,2048]{1,0:T(8,128)(2,1)} %param.17, f32[2048]{0:T(1024)S(1)} %copy-done.5, f32[512]{0:T(512)S(1)} %add_rsqrt_fusion), kind=kOutput, calls=%fused_computation.105 | convolution fusion | flops 272629760 | bytes 2893824 | tf_op jit(solution)/shard_map/dot_general | solution.py:70
  110.9 4.0 %collective-permute-start.1 = (bf16[128,2,64]{0,2,1:T(8,128)(2,1)S(1)}, bf16[128,2,64]{0,2,1:T(8,128)(2,1)}, u32[]{:S(2)}, u32[]{:S(2)}) collective-permute-start(bf16[128,2,64]{0,2,1:T(8,128)(2,1)S(1)} %pad_maximum_fusion.1), channel_id=1, source_target_pairs={{0,4},{4,8},{8,12},{12,16},{16,20},{20,24},{24,28},{1,5},{5,9},{9,... | collective-permute-start | bytes 98312 | tf_op jit(solution)/shard_map/ppermute | solution.py:16
  114.8 2.1 %convolution_convert_fusion.3 = bf16[512,128]{0,1:T(8,128)(2,1)S(1)} fusion(bf16[2048,128]{1,0:T(8,128)(2,1)} %param.21, bf16[512,2048]{1,0:T(8,128)(2,1)S(1)} %copy-done.1, f32[2048]{0:T(1024)S(1)} %copy-done.5, f32[512]{0:T(512)S(1)} %add_rsqrt_fusion), kind=kOutput, calls=%fused_computation.43 | convolution fusion | flops 272695296 | bytes 2762752 | tf_op jit(solution)/shard_map/dot_general | solution.py:76
  116.9 3.6 %collective-permute-start = (bf16[128,2,64]{0,2,1:T(8,128)(2,1)S(1)}, bf16[128,2,64]{0,2,1:T(8,128)(2,1)}, u32[]{:S(2)}, u32[]{:S(2)}) collective-permute-start(bf16[128,2,64]{0,2,1:T(8,128)(2,1)S(1)} %bitcast.128), channel_id=1, source_target_pairs={{0,4},{4,8},{8,12},{12,16},{16,20},{20,24},{24,28},{1,5},{5,9},{9,... | collective-permute-start | bytes 98312 | tf_op jit(solution)/shard_map/ppermute | solution.py:16
  120.5 2.5 %fusion.68 = f32[512,256]{0,1:T(8,128)S(1)} fusion(bf16[2048,256]{1,0:T(8,128)(2,1)S(1)} %copy-done.3, bf16[512,2048]{1,0:T(8,128)(2,1)} %param.17, f32[2048]{0:T(1024)S(1)} %copy-done.5, f32[512]{0:T(512)S(1)} %add_rsqrt_fusion), kind=kOutput, calls=%fused_computation.104 | convolution fusion | flops 541065216 | bytes 3680256 | tf_op jit(solution)/shard_map/dot_general | solution.py:64
  123.0 0.1 subtract_convert_fusion
  123.1 0.4 fusion.30
  123.6 0.1 max.22
  123.6 1.8 fusion.10
  125.5 0.1 broadcast_maximum_fusion
  125.6 1.1 fusion
  126.7 0.1 exponential_add_fusion
  126.8 2.4 %fusion.31 = bf16[2,64,2,512]{3,1,2,0:T(8,128)(2,1)S(1)} fusion(f32[2,640,512,2]{2,1,3,0:T(8,128)S(1)} %get-tuple-element.32, f32[2,2,512]{2,1,0:T(2,128)S(1)} %exponential_add_fusion, f32[2,2,512]{2,1,0:T(2,128)S(1)} %broadcast_maximum_fusion, pred[512,640]{0,1:T(8,128)(4,1)S(1)} %fusion.30, bf16[512,2,64]{0,2,1:T(8,128)(2,1)S(1)} %bitcast.129, ...), kind=kOutput, calls=%fused_computation.41 | convolution fusion | flops 174784512 | bytes 6012928 | tf_op jit(solution)/shard_map/while/body/eval_jaxpr/hgqk,khd->qhgd/dot_general | solution.py:108
  129.2 2.1 %convolution_convert_fusion = bf16[512,2048]{1,0:T(8,128)(2,1)} fusion(bf16[512,256]{0,1:T(8,128)(2,1)S(1)} %bitcast.123, bf16[256,2048]{1,0:T(8,128)(2,1)S(1)} %copy-done), kind=kOutput, calls=%fused_computation.20 | convolution fusion | flops 537919488 | bytes 3407872 | tf_op jit(solution)/shard_map/dot_general | solution.py:117
  131.3 0.0 reduce-scatter.3.cloned.1.call-update
  131.4 22.1 %reduce-scatter.5.cloned.1.call-done = bf16[512,1152]{0,1:T(8,128)(2,1)} async-done(((bf16[2048,1152]{0,1:T(8,128)(2,1)}), bf16[512,1152]{0,1:T(8,128)(2,1)}) %reduce-scatter.5.cloned.1.call-update) | async-done | bytes 1179664 | tf_op jit(solution)/shard_map/reduce_scatter | solution.py:161
  153.5 1.3 slice.32
  154.8 30.9 %all_to_all.25 = bf16[512,8,128]{0,2,1:T(8,128)(2,1)S(1)} all-to-all(bf16[512,8,128]{0,2,1:T(8,128)(2,1)S(1)} %bitcast.122), channel_id=1, replica_groups=mesh['ep'=8,'tp'=4] {'ep'}, dimensions={1} | all-to-all | bytes 2097152 | tf_op jit(solution)/shard_map/all_to_all | solution.py:168
  185.7 2.3 %fusion.32 = bf16[128,512]{1,0:T(8,128)(2,1)} fusion(f32[1024,128]{1,0:T(8,128)S(1)} %get-tuple-element.17, bf16[512,1024]{0,1:T(8,128)(2,1)S(1)} %bitcast.119, bf16[512,1152]{0,1:T(8,128)(2,1)} %reduce-scatter.5.cloned.1.call-done), kind=kOutput, calls=%fused_computation.44 | convolution fusion | flops 805502976 | bytes 1835008 | tf_op jit(solution)/shard_map/dot_general | solution.py:169
  (29 shorter events, 0.2 us)
Async XLA Ops:
  7.2 122.1 %copy-start = (bf16[256,2048]{1,0:T(8,128)(2,1)S(1)}, bf16[256,2048]{1,0:T(8,128)(2,1)}, u32[]{:S(2)}) copy-start(bf16[256,2048]{1,0:T(8,128)(2,1)} %param.23) | copy-start | bytes 3145732
  7.2 40.7 %copy-start.2 = (bf16[2048,256]{1,0:T(8,128)(2,1)S(1)}, bf16[2048,256]{1,0:T(8,128)(2,1)}, u32[]{:S(2)}) copy-start(bf16[2048,256]{1,0:T(8,128)(2,1)} %param.31) | copy-start | bytes 3145732
  7.2 74.3 %all-gather.2.cloned.1.call-start = ((), (), s32[]{:S(2)}) async-start(), calls=%async_computation.5 | async-start | bytes 5242880 | tf_op jit(solution)/shard_map/all_gather | solution.py:145
  47.8 105.6 %reduce-scatter.5.cloned.1.call-start = ((), (), s32[]{:S(2)}) async-start(), calls=%async_computation.6 | async-start | bytes 5898240 | tf_op jit(solution)/shard_map/reduce_scatter | solution.py:161
  105.5 2.7 %copy-start.4 = (bf16[2048,128]{1,0:T(8,128)(2,1)S(1)}, bf16[2048,128]{1,0:T(8,128)(2,1)}, u32[]{:S(2)}) copy-start(bf16[2048,128]{1,0:T(8,128)(2,1)} %param.20) | copy-start | bytes 1572868
  105.5 2.7 %copy-start.5 = (f32[2048]{0:T(1024)S(1)}, f32[2048]{0:T(1024)}, u32[]{:S(2)}) copy-start(f32[2048]{0:T(1024)} %param.18) | copy-start | bytes 24580
  105.5 82.5 %reduce-scatter.3.cloned.1.call-start = ((), (), s32[]{:S(2)}) async-start(), calls=%async_computation.4 | async-start | bytes 2621440 | tf_op jit(solution)/shard_map/reduce_scatter | solution.py:116
  105.6 9.3 %copy-start.1 = (bf16[512,2048]{1,0:T(8,128)(2,1)S(1)}, bf16[512,2048]{1,0:T(8,128)(2,1)}, u32[]{:S(2)}) copy-start(bf16[512,2048]{1,0:T(8,128)(2,1)} %param.17) | copy-start | bytes 6291460
  108.2 12.3 %copy-start.3 = (bf16[2048,256]{1,0:T(8,128)(2,1)S(1)}, bf16[2048,256]{1,0:T(8,128)(2,1)}, u32[]{:S(2)}) copy-start(bf16[2048,256]{1,0:T(8,128)(2,1)} %param.19) | copy-start | bytes 3145732
  110.9 12.8 %collective-permute-start.1 = (bf16[128,2,64]{0,2,1:T(8,128)(2,1)S(1)}, bf16[128,2,64]{0,2,1:T(8,128)(2,1)}, u32[]{:S(2)}, u32[]{:S(2)}) collective-permute-start(bf16[128,2,64]{0,2,1:T(8,128)(2,1)S(1)} %pad_maximum_fusion.1), channel_id=1, source_target_pairs={{0,4},{4,8},{8,12},{12,16},{16,20},{20,24},{24,28},{1,5},{5,9},{9,... | collective-permute-start | bytes 98312 | tf_op jit(solution)/shard_map/ppermute | solution.py:16
  116.9 6.7 %copy-start.6 = (f32[4]{0:T(128)S(1)}, f32[4]{0:T(128)}, u32[]{:S(2)}) copy-start(f32[4]{0:T(128)} %param.22) | copy-start | bytes 52
  116.9 9.9 %collective-permute-start = (bf16[128,2,64]{0,2,1:T(8,128)(2,1)S(1)}, bf16[128,2,64]{0,2,1:T(8,128)(2,1)}, u32[]{:S(2)}, u32[]{:S(2)}) collective-permute-start(bf16[128,2,64]{0,2,1:T(8,128)(2,1)S(1)} %bitcast.128), channel_id=1, source_target_pairs={{0,4},{4,8},{8,12},{12,16},{16,20},{20,24},{24,28},{1,5},{5,9},{9,... | collective-permute-start | bytes 98312 | tf_op jit(solution)/shard_map/ppermute | solution.py:16
Sparse Core Ops, SparseCore 0:
  48.0 33.4 all-gather.1
  105.6 47.7 reduce-scatter.4
  156.6 31.1 reduce-scatter.2
where the time goes:
time: 195 us
  blocking collectives  63.9 us (33%)
  waiting for transfers between devices  53.1 us (27%)
  matrix products  37.9 us (19%)
  between operations  14 us (7%)
  other arithmetic  12.5 us (6%)
  starting transfers between devices  7.63 us (4%)
  local copies, waits for them, and re-layouts  5.45 us (3%)
    all_to_all x1, blocking collectives, local(): lax.all_to_all(outgoing, 'ep', split_axis=0, concat_axis=0, tiled=True)  32.9 us
    all_gather x1, waiting for transfers between devices, local(): piece = lax.all_gather(arrived, 'tp', axis=1, tiled=True)  30.9 us
    all_to_all x1, blocking collectives, local(): lax.all_to_all(routed_part, 'ep', split_axis=1, concat_axis=1, tiled=True)  30.9 us
    reduce_scatter x1, waiting for transfers between devices, local(): lax.psum_scatter(jnp.concatenate([routed_term, shared_term], axis=1).asty...  22.1 us
    dot_general x1, matrix products, local(): jnp.einsum('sjcf,jfd->dsjc', hidden, w_down_exp, preferred_element_type=j...  11.8 us
    ppermute x2, starting transfers between devices, from_behind(): return lax.ppermute(value, axis, pairs)  7.51 us
    dot_general x1, matrix products, local(): jnp.einsum('sjcd,jdf->sjcf', part, w_gate_exp, preferred_element_type=jnp...  7.19 us
  transfers between devices with their start and end apart: 5, of which 2 were waited for; matrix products, arithmetic and copies ran while one was open for 12% of the time, Pallas kernels for 0%

commit v1 on v0

--- a/solution.py
+++ b/solution.py
@@ -8,6 +8,12 @@
 BAND_LENGTH = 128
 rope_base = 10000.0
 norm_eps = 1e-06
+
+
+def supply_all_shelves_here(frame):
+    raw_out = jnp.stack([frame for _ in range(lax.axis_size("tp"))], axis=0)
+    q_next = lax.all_to_all(raw_out, "tp", 0, 0)
+    return jnp.concatenate(q_next, 1)
 
 
 def from_behind(value, axis, by):
@@ -142,7 +148,7 @@
         jnp.bfloat16
     )
     arrived = lax.all_to_all(outgoing, "ep", split_axis=0, concat_axis=0, tiled=True)
-    piece = lax.all_gather(arrived, "tp", axis=1, tiled=True)
+    piece = supply_all_shelves_here(arrived)
     cols = piece.shape[1]
     part = piece.reshape(n_expdev, exp_dev, capacity, cols)
     gate_pre = jnp.einsum("sjcd,jdf->sjcf", part, w_gate_exp, preferred_element_type=jnp.float32)

time: 195 us -> 230 us (1.18)
  local copies, waits for them, and re-layouts: 5.45 us -> 22.8 us
  waiting for transfers between devices: 53.1 us -> 66.8 us
  starting transfers between devices: 7.63 us -> 11.1 us
    all_to_all x0 -> x1, waiting for transfers between devices: none -> 44.1 us  [supply_all_shelves_here(): q_next = lax.all_to_all(raw_out, 'tp', 0, 0)]
    all_gather x1 -> x0, waiting for transfers between devices: 30.9 us -> none  [local(): piece = lax.all_gather(arrived, 'tp', axis=1, tiled=True)]
    another operation x1 -> x3, local copies, waits for them, and re-layouts: 0.01 us -> 10 us  [the longest x1 7.75 us: local(): part = piece.reshape(n_expdev, exp_dev, capacity, cols)]
    reshape x0 -> x1, local copies, waits for them, and re-layouts: none -> 7.39 us  [supply_all_shelves_here(): return jnp.concatenate(q_next, 1)]
    all_to_all x0 -> x1, starting transfers between devices: none -> 4.86 us  [supply_all_shelves_here(): q_next = lax.all_to_all(raw_out, 'tp', 0, 0)]
  transfers between devices with their start and end apart: 5 -> 5, of which waited for: 2 -> 2; matrix products, arithmetic and copies ran while one was open for 12% -> 11% of each run, Pallas kernels for 0% -> 0%
where the time goes in v1:
time: 230 us
  waiting for transfers between devices  66.8 us (29%)
  blocking collectives  63.7 us (28%)
  matrix products  38.3 us (17%)
  local copies, waits for them, and re-layouts  22.8 us (10%)
  between operations  14.3 us (6%)
  other arithmetic  12.5 us (5%)
  starting transfers between devices  11.1 us (5%)
    all_to_all x1, waiting for transfers between devices, supply_all_shelves_here(): q_next = lax.all_to_all(raw_out, 'tp', 0, 0)  44.1 us
    all_to_all x1, blocking collectives, local(): lax.all_to_all(outgoing, 'ep', split_axis=0, concat_axis=0, tiled=True)  32.8 us
    all_to_all x1, blocking collectives, local(): lax.all_to_all(routed_part, 'ep', split_axis=1, concat_axis=1, tiled=True)  30.9 us
    reduce_scatter x1, waiting for transfers between devices, local(): lax.psum_scatter(jnp.concatenate([routed_term, shared_term], axis=1).asty...  22.6 us
    dot_general x1, matrix products, local(): jnp.einsum('sjcf,jfd->dsjc', hidden, w_down_exp, preferred_element_type=j...  11.8 us
    another operation x1, local copies, waits for them, and re-layouts, local(): part = piece.reshape(n_expdev, exp_dev, capacity, cols)  7.75 us
    reshape x1, local copies, waits for them, and re-layouts, supply_all_shelves_here(): return jnp.concatenate(q_next, 1)  7.39 us
    dot_general x1, matrix products, local(): jnp.einsum('sjcd,jdf->sjcf', part, w_gate_exp, preferred_element_type=jnp...  7.19 us
  transfers between devices with their start and end apart: 5, of which 2 were waited for; matrix products, arithmetic and copies ran while one was open for 11% of the time, Pallas kernels for 0%

profile of v1, /device:TPU:0, one launch (start us, length us, event | category | flops | bytes accessed | tf_op | source)
XLA Modules:
  0.0 229.6 jit_solution(14351808855409867024)
XLA Ops:
  7.2 0.9 copy.54
  8.1 0.1 eq.40
  8.2 0.1 eq.44
  8.3 1.2 reduce-window.6
  9.4 0.2 slice_reduce_fusion
  9.7 0.1 fusion.58
  9.8 0.1 reduce_sum.60
  9.9 0.1 copy.57
  10.0 0.7 multiply_add_fusion
  10.7 1.2 fusion.34
  11.9 1.2 convert_reduce_fusion
  13.1 1.2 fusion.36
  14.3 0.4 convolution_convert_fusion.2
  14.8 32.8 %all_to_all.26 = bf16[8,128,512]{2,1,0:T(8,128)(2,1)S(1)} all-to-all(bf16[8,128,512]{2,1,0:T(8,128)(2,1)S(1)} %bitcast.121), channel_id=1, replica_groups=mesh['ep'=8,'tp'=4] {'ep'}, dimensions={0} | all-to-all | bytes 2097152 | tf_op jit(solution)/shard_map/all_to_all | solution.py:150
  47.6 2.3 stack.10
  49.9 4.9 %all-to-all-start.1 = ((bf16[4,1024,512]{2,1,0:T(8,128)(2,1)}), bf16[4,1024,512]{2,1,0:T(8,128)(2,1)}, u32[]{:S(2)}, u32[]{:S(2)}) async-start(bf16[4,1024,512]{2,1,0:T(8,128)(2,1)} %stack.10), calls=%async_computation.2 | async-start | bytes 8388608 | tf_op jit(solution)/shard_map/all_to_all | solution.py:15
  54.8 0.2 reduce-scatter.5.cloned.1.call-start
  55.0 1.5 fusion.73
  56.5 2.3 %fusion.16 = bf16[2048,128]{0,1:T(8,128)(2,1)S(1)} fusion(bf16[256,2048]{1,0:T(8,128)(2,1)} %param.33, bf16[128,2048]{1,0:T(8,128)(2,1)S(1)} %fusion.36, bf16[2048,256]{1,0:T(8,128)(2,1)} %param.32, f32[128,256]{1,0:T(8,128)S(1)} %fusion.73), kind=kOutput, calls=%fused_computation.23 | convolution fusion | flops 268894208 | bytes 3276800 | tf_op jit(solution)/shard_map/dot_general | solution.py:164
  58.9 44.1 %all-to-all-done.1 = bf16[4,1024,512]{2,1,0:T(8,128)(2,1)} async-done(((bf16[4,1024,512]{2,1,0:T(8,128)(2,1)}), bf16[4,1024,512]{2,1,0:T(8,128)(2,1)}, u32[]{:S(2)}, u32[]{:S(2)}) %all-to-all-start.1) | async-done | bytes 4194336 | tf_op jit(solution)/shard_map/all_to_all | solution.py:15
  103.0 7.4 %copy.58 = bf16[1024,4,512]{2,1,0:T(4,128)(2,1)} copy(bf16[1024,4,512]{2,0,1:T(8,128)(2,1)} %bitcast.16) | data formatting | bytes 8388608 | tf_op jit(solution)/shard_map/reshape | solution.py:16
  110.4 7.7 %reshape_reshape.3 = bf16[8,2,64,2048]{3,2,1,0:T(8,128)(2,1)} reshape(bf16[1024,4,512]{2,1,0:T(4,128)(2,1)} %copy.58) | data formatting | bytes 8388608 | tf_op jit(solution)/shard_map/reshape;reshape | solution.py:153
  118.1 7.2 %fusion.8 = f32[2,8,64,512]{3,2,1,0:T(8,128)} fusion(bf16[2,2048,512]{2,1,0:T(8,128)(2,1)} %param.28, bf16[8,2,64,2048]{3,2,1,0:T(8,128)(2,1)} %reshape_reshape.3), kind=kOutput, calls=%fused_computation.14 | convolution fusion | flops 2147483648 | bytes 10485760 | tf_op jit(solution)/shard_map/sjcd,jdf->sjcf/dot_general | solution.py:154
  125.3 11.8 %convert_bitcast_fusion = bf16[2048,8,2,64]{0,3,1,2:T(8,128)(2,1)} fusion(bf16[2,512,2048]{2,1,0:T(8,128)(2,1)} %param.30, f32[2,8,64,512]{3,2,1,0:T(8,128)} %fusion.8, bf16[2,2048,512]{2,1,0:T(8,128)(2,1)} %param.29, bf16[8,2,64,2048]{3,2,1,0:T(8,128)(2,1)} %reshape_reshape.3), kind=kOutput, calls=%fused_computation.16 | convolution fusion | flops 4300210176 | bytes 18874368 | tf_op jit(solution)/shard_map/sjcf,jfd->dsjc/dot_general | solution.py:161
  137.1 2.5 %copy.61 = bf16[2048,8,2,64]{0,3,2,1:T(8,128)(2,1)S(1)} copy(bf16[2048,8,2,64]{0,3,1,2:T(8,128)(2,1)} %convert_bitcast_fusion) | data formatting | bytes 8388608 | tf_op jit(solution)/shard_map/sjcf,jfd->dsjc/transpose | solution.py:161
  139.6 2.5 %pad_maximum_fusion = bf16[2048,1152]{0,1:T(8,128)(2,1)} fusion(bf16[2048,128]{0,1:T(8,128)(2,1)S(1)} %fusion.16, bf16[2048,1024]{0,1:T(8,128)(2,1)S(1)} %bitcast.118), kind=kLoop, calls=%fused_computation.5 | loop fusion | flops 9437184 | bytes 9437184 | tf_op jit(solution)/shard_map/concatenate | solution.py:168
  142.1 0.0 reduce-scatter.5.cloned.1.call-update
  142.1 0.0 reduce-scatter.3.cloned.1.call-start
  142.2 2.2 fusion.1
  144.5 0.3 multiply_cosine_fusion
  144.8 3.1 %fusion.70 = f32[512,128]{0,1:T(8,128)S(1)} fusion(bf16[2048,128]{1,0:T(8,128)(2,1)S(1)} %copy-done.2, bf16[512,2048]{1,0:T(8,128)(2,1)} %param.17, f32[2048]{0:T(1024)S(1)} %copy-done.3, f32[512]{0:T(512)S(1)} %add_rsqrt_fusion), kind=kOutput, calls=%fused_computation.105 | convolution fusion | flops 272629760 | bytes 2893824 | tf_op jit(solution)/shard_map/dot_general | solution.py:76
  148.0 3.2 %collective-permute-start.1 = (bf16[128,2,64]{0,2,1:T(8,128)(2,1)S(1)}, bf16[128,2,64]{0,2,1:T(8,128)(2,1)S(1)}, u32[]{:S(2)}, u32[]{:S(2)}) collective-permute-start(bf16[128,2,64]{0,2,1:T(8,128)(2,1)S(1)} %pad_maximum_fusion.1), channel_id=1, source_target_pairs={{0,4},{4,8},{8,12},{12,16},{16,20},{20,24},{24,28},{1,5},{5,9},{9,... | collective-permute-start | bytes 98312 | tf_op jit(solution)/shard_map/ppermute | solution.py:22
  151.2 2.0 convolution_convert_fusion.3
  153.2 2.8 %collective-permute-start = (bf16[128,2,64]{0,2,1:T(8,128)(2,1)S(1)}, bf16[128,2,64]{0,2,1:T(8,128)(2,1)S(1)}, u32[]{:S(2)}, u32[]{:S(2)}) collective-permute-start(bf16[128,2,64]{0,2,1:T(8,128)(2,1)S(1)} %bitcast.128), channel_id=1, source_target_pairs={{0,4},{4,8},{8,12},{12,16},{16,20},{20,24},{24,28},{1,5},{5,9},{9,... | collective-permute-start | bytes 98312 | tf_op jit(solution)/shard_map/ppermute | solution.py:22
  156.0 2.8 %fusion.68 = f32[512,256]{0,1:T(8,128)S(1)} fusion(bf16[2048,256]{1,0:T(8,128)(2,1)} %param.19, bf16[512,2048]{1,0:T(8,128)(2,1)} %param.17, f32[2048]{0:T(1024)S(1)} %copy-done.3, f32[512]{0:T(512)S(1)} %add_rsqrt_fusion), kind=kOutput, calls=%fused_computation.104 | convolution fusion | flops 541065216 | bytes 3680256 | tf_op jit(solution)/shard_map/dot_general | solution.py:70
  158.8 0.1 subtract_convert_fusion
  158.9 0.4 fusion.30
  159.3 0.1 max.22
  159.4 1.1 fusion.10
  160.5 0.1 broadcast_maximum_fusion
  160.6 1.1 fusion
  161.7 0.1 exponential_add_fusion
  161.8 1.6 fusion.31
  163.5 2.1 convolution_convert_fusion
  165.6 22.6 %reduce-scatter.5.cloned.1.call-done = bf16[512,1152]{0,1:T(8,128)(2,1)} async-done(((bf16[2048,1152]{0,1:T(8,128)(2,1)}), bf16[512,1152]{0,1:T(8,128)(2,1)}) %reduce-scatter.5.cloned.1.call-update) | async-done | bytes 1179664 | tf_op jit(solution)/shard_map/reduce_scatter | solution.py:167
  188.2 1.3 slice.32
  189.5 30.9 %all_to_all.27 = bf16[512,8,128]{0,2,1:T(8,128)(2,1)S(1)} all-to-all(bf16[512,8,128]{0,2,1:T(8,128)(2,1)S(1)} %bitcast.122), channel_id=1, replica_groups=mesh['ep'=8,'tp'=4] {'ep'}, dimensions={1} | all-to-all | bytes 2097152 | tf_op jit(solution)/shard_map/all_to_all | solution.py:174
  220.4 2.3 %fusion.32 = bf16[128,512]{1,0:T(8,128)(2,1)} fusion(f32[1024,128]{1,0:T(8,128)S(1)} %get-tuple-element.17, bf16[512,1024]{0,1:T(8,128)(2,1)S(1)} %bitcast.120, bf16[512,1152]{0,1:T(8,128)(2,1)} %reduce-scatter.5.cloned.1.call-done), kind=kOutput, calls=%fused_computation.44 | convolution fusion | flops 805502976 | bytes 1835008 | tf_op jit(solution)/shard_map/dot_general | solution.py:175
  (27 shorter events, 0.2 us)
Async XLA Ops:
  7.2 156.3 %copy-start = (bf16[256,2048]{1,0:T(8,128)(2,1)S(1)}, bf16[256,2048]{1,0:T(8,128)(2,1)}, u32[]{:S(2)}) copy-start(bf16[256,2048]{1,0:T(8,128)(2,1)} %param.23) | copy-start | bytes 3145732
  49.9 53.1 %all-to-all-start.1 = ((bf16[4,1024,512]{2,1,0:T(8,128)(2,1)}), bf16[4,1024,512]{2,1,0:T(8,128)(2,1)}, u32[]{:S(2)}, u32[]{:S(2)}) async-start(bf16[4,1024,512]{2,1,0:T(8,128)(2,1)} %stack.10), calls=%async_computation.2 | async-start | bytes 8388608 | tf_op jit(solution)/shard_map/all_to_all | solution.py:15
  54.8 133.5 %reduce-scatter.5.cloned.1.call-start = ((), (), s32[]{:S(2)}) async-start(), calls=%async_computation.6 | async-start | bytes 5898240 | tf_op jit(solution)/shard_map/reduce_scatter | solution.py:167
  142.1 2.7 %copy-start.2 = (bf16[2048,128]{1,0:T(8,128)(2,1)S(1)}, bf16[2048,128]{1,0:T(8,128)(2,1)}, u32[]{:S(2)}) copy-start(bf16[2048,128]{1,0:T(8,128)(2,1)} %param.20) | copy-start | bytes 1572868
  142.1 2.7 %copy-start.3 = (f32[2048]{0:T(1024)S(1)}, f32[2048]{0:T(1024)}, u32[]{:S(2)}) copy-start(f32[2048]{0:T(1024)} %param.18) | copy-start | bytes 24580
  142.1 80.6 %reduce-scatter.3.cloned.1.call-start = ((), (), s32[]{:S(2)}) async-start(), calls=%async_computation.5 | async-start | bytes 2621440 | tf_op jit(solution)/shard_map/reduce_scatter | solution.py:122
  142.2 9.0 %copy-start.1 = (bf16[512,2048]{1,0:T(8,128)(2,1)S(1)}, bf16[512,2048]{1,0:T(8,128)(2,1)}, u32[]{:S(2)}) copy-start(bf16[512,2048]{1,0:T(8,128)(2,1)} %param.17) | copy-start | bytes 6291460
  148.0 11.5 %collective-permute-start.1 = (bf16[128,2,64]{0,2,1:T(8,128)(2,1)S(1)}, bf16[128,2,64]{0,2,1:T(8,128)(2,1)S(1)}, u32[]{:S(2)}, u32[]{:S(2)}) collective-permute-start(bf16[128,2,64]{0,2,1:T(8,128)(2,1)S(1)} %pad_maximum_fusion.1), channel_id=1, source_target_pairs={{0,4},{4,8},{8,12},{12,16},{16,20},{20,24},{24,28},{1,5},{5,9},{9,... | collective-permute-start | bytes 98312 | tf_op jit(solution)/shard_map/ppermute | solution.py:22
  153.2 6.2 %copy-start.4 = (f32[4]{0:T(128)S(1)}, f32[4]{0:T(128)}, u32[]{:S(2)}) copy-start(f32[4]{0:T(128)} %param.22) | copy-start | bytes 52
  153.2 8.6 %collective-permute-start = (bf16[128,2,64]{0,2,1:T(8,128)(2,1)S(1)}, bf16[128,2,64]{0,2,1:T(8,128)(2,1)S(1)}, u32[]{:S(2)}, u32[]{:S(2)}) collective-permute-start(bf16[128,2,64]{0,2,1:T(8,128)(2,1)S(1)} %bitcast.128), channel_id=1, source_target_pairs={{0,4},{4,8},{8,12},{12,16},{16,20},{20,24},{24,28},{1,5},{5,9},{9,... | collective-permute-start | bytes 98312 | tf_op jit(solution)/shard_map/ppermute | solution.py:22
Sparse Core Ops, SparseCore 0:
  142.3 45.9 reduce-scatter.4
  191.3 31.1 reduce-scatter.2
